TPU v7x, 32 devices: a whole 2x2x4 slice. The times are simulated.
32 devices in a mesh: sp: 8 (over z, x), tp: 4 (over y, core).
Axes of the slice: x: 2, y: 2, z: 4, core: 2. Of those that a mesh axis runs over, the one named last changes fastest.
Arguments:
- tokens: bfloat16 [1536, 2048], P(('sp', 'tp')), may hold values from -54 to 54
- w_query: bfloat16 [2048, 2048], P(None, 'tp'), may hold values from -0.21875 to 0.21875
- w_key: bfloat16 [2048, 2048], P(None, 'tp'), may hold values from -0.125 to 0.125
- w_value: bfloat16 [2048, 2048], P(None, 'tp'), may hold values from -0.125 to 0.125
- w_out: bfloat16 [2048, 2048], P('tp'), may hold values from -0.125 to 0.125
- mix_weight: float32 [16], P('tp'), may hold values from 0.3 to 0.8
- out_gain: float32 [128], replicated, may hold values from 0.1 to 1.9
Outputs:
- mixed: bfloat16 [1536, 2048], P(('sp', 'tp'))
All inputs are finite; a program needn't handle non-finite values.
Results may differ from a plain program's by a relative error of at most 0.018.
The roundings to bfloat16 on the way count: a program that leaves them out, or rounds other values in their place, can miss the bound.
Values may be sent and summed in bfloat16 or wider, within the bound.
A program may use at most 192 MiB of HBM per device.

v0:
```python
import jax
import jax.numpy as jnp
from jax import lax
from jax.sharding import PartitionSpec as P


def block_rows(rows):
    best = 1
    for candidate in range(1, rows + 1):
        if rows % candidate == 0 and candidate <= 2048:
            best = candidate
    return best


def shards(tokens, w_query, w_key, w_value, w_out, mix_weight, out_gain):
    query_cols = w_query.shape[1]
    key_cols = w_key.shape[1]
    heads_here = mix_weight.shape[0]
    head_dim = query_cols // (2 * heads_here)
    value_dim = w_value.shape[1] // heads_here
    piece = lax.all_gather(tokens, "tp", axis=0, tiled=True)
    part_q = jnp.dot(piece, w_query, preferred_element_type=jnp.float32).astype(jnp.bfloat16)
    part_k = jnp.dot(piece, w_key, preferred_element_type=jnp.float32).astype(jnp.bfloat16)
    part_v = jnp.dot(piece, w_value, preferred_element_type=jnp.float32).astype(jnp.bfloat16)
    joined = jnp.concatenate([part_q, part_k, part_v], axis=1)
    queries = joined[:, :query_cols]
    keys = joined[:, query_cols : query_cols + key_cols]
    values = joined[:, query_cols + key_cols :]
    n_query = queries.shape[0]
    query_four = queries.reshape(n_query, heads_here, 2, head_dim)
    scale = head_dim ** (-0.5)

    def step(carry, block):
        running_max, running_sum, accum = carry
        key_blk, value_blk = block
        scores = (
            jnp.einsum("qhmd,khmd->hmqk", query_four, key_blk, preferred_element_type=jnp.float32)
            * scale
        )
        new_max = jnp.maximum(running_max, jnp.max(scores, axis=-1))
        factor = jnp.exp(running_max - new_max)
        expw = jnp.exp(scores - new_max[..., None])
        running_sum = running_sum * factor + jnp.sum(expw, axis=-1)
        weights = expw.astype(jnp.bfloat16)
        accum = accum * factor[..., None] + jnp.einsum(
            "hmqk,khe->hmqe", weights, value_blk, preferred_element_type=jnp.float32
        )
        return ((new_max, running_sum, accum), None)

    initial = (
        jnp.full((heads_here, 2, n_query), -1e30, jnp.float32),
        jnp.zeros((heads_here, 2, n_query), jnp.float32),
        jnp.zeros((heads_here, 2, n_query, value_dim), jnp.float32),
    )
    all_keys, all_values = (
        lax.all_gather(keys, "sp", axis=0, tiled=True),
        lax.all_gather(values, "sp", axis=0, tiled=True),
    )
    carry = initial
    rows = all_keys.shape[0]
    group = block_rows(rows)
    key_blocks = all_keys.reshape(rows // group, group, heads_here, 2, head_dim)
    value_blocks = all_values.reshape(rows // group, group, heads_here, value_dim)
    carry, unused = lax.scan(step, carry, (key_blocks, value_blocks))
    running_max, running_sum, accum = carry
    heads_out = (
        accum[:, 0] / running_sum[:, 0, :, None]
        - mix_weight[:, None, None] * accum[:, 1] / running_sum[:, 1, :, None]
    )
    meansq = jnp.mean(heads_out * heads_out, axis=-1, keepdims=True)
    normed = (heads_out * lax.rsqrt(meansq + 1e-06) * out_gain).astype(jnp.bfloat16)
    normed = normed.transpose(1, 0, 2).reshape(n_query, heads_here * value_dim)
    return lax.psum_scatter(
        jnp.dot(normed, w_out, preferred_element_type=jnp.float32).astype(jnp.bfloat16),
        "tp",
        scatter_dimension=0,
        tiled=True,
    )


def solution(mesh):
    in_specs = (
        P(("sp", "tp"), None),
        P(None, "tp"),
        P(None, "tp"),
        P(None, "tp"),
        P("tp", None),
        P("tp"),
        P(),
    )
    out_specs = P(("sp", "tp"), None)
    return jax.shard_map(shards, mesh=mesh, in_specs=in_specs, out_specs=out_specs, check_vma=False)
```

profile of v0, /device:TPU:0, one launch (start us, length us, event | category | flops | bytes accessed | tf_op | source)
XLA Modules:
  0.0 149.1 jit_solution(17740155606464620466)
XLA Ops:
  6.5 0.0 copy-start
  6.5 0.0 all-gather.3.cloned.1.call-start
  6.5 10.4 %all_gather.9 = bf16[192,2048]{1,0:T(8,128)(2,1)S(1)} all-gather(bf16[48,2048]{1,0:T(8,128)(2,1)} %param.7), channel_id=1, replica_groups=mesh['sp'=8,'tp'=4] {'tp'}, dimensions={0}, use_global_device_ids=true | all-gather | bytes 983040 | tf_op jit(solution)/shard_map/all_gather | solution.py:21
  17.0 2.8 %convolution_convert_fusion.2 = bf16[192,512]{1,0:T(8,128)(2,1)} fusion(bf16[192,2048]{1,0:T(8,128)(2,1)S(1)} %all_gather.9, bf16[2048,512]{1,0:T(8,128)(2,1)} %param.9), kind=kOutput, calls=%fused_computation.11 | convolution fusion | flops 402751488 | bytes 3080192 | tf_op jit(solution)/shard_map/dot_general | solution.py:23
  19.8 0.0 all-gather.3.cloned.1.call-update
  19.8 0.0 all-gather.5.cloned.1.call-start
  19.9 2.9 %convolution_convert_fusion.1 = bf16[192,512]{1,0:T(8,128)(2,1)} fusion(bf16[192,2048]{1,0:T(8,128)(2,1)S(1)} %all_gather.9, bf16[2048,512]{1,0:T(8,128)(2,1)} %param.10), kind=kOutput, calls=%fused_computation.10 | convolution fusion | flops 402751488 | bytes 3080192 | tf_op jit(solution)/shard_map/dot_general | solution.py:24
  22.7 0.0 all-gather.5.cloned.1.call-update
  22.8 0.0 reduce-scatter.2.cloned.1.call-start
  22.8 2.2 %convolution_convert_fusion.3 = bf16[192,512]{1,0:T(8,128)(2,1)S(1)} fusion(bf16[192,2048]{1,0:T(8,128)(2,1)S(1)} %all_gather.9, bf16[2048,512]{1,0:T(8,128)(2,1)} %param.8), kind=kOutput, calls=%fused_computation.12 | convolution fusion | flops 402751488 | bytes 3080192 | tf_op jit(solution)/shard_map/dot_general | solution.py:22
  25.0 0.1 copy.12
  25.1 39.9 %all-gather.3.cloned.1.call-done = bf16[1536,512]{1,0:T(8,128)(2,1)} async-done(((bf16[192,512]{1,0:T(8,128)(2,1)}), bf16[1536,512]{1,0:T(8,128)(2,1)}) %all-gather.3.cloned.1.call-update) | async-done | bytes 1572880 | tf_op jit(solution)/shard_map/all_gather | solution.py:56
  65.0 2.6 %copy.13 = bf16[1536,512]{0,1:T(8,128)(2,1)} copy(bf16[1536,512]{1,0:T(8,128)(2,1)} %all-gather.3.cloned.1.call-done) | data formatting | bytes 3145728 | tf_op jit(solution)/shard_map/all_gather | solution.py:56
  67.6 2.9 %multiply_reduce_fusion = (f32[4,2,192]{2,1,0:T(2,128)S(1)}, f32[4,2,192,1536]{3,2,1,0:T(8,128)S(1)}) fusion(bf16[192,4,2,64]{0,3,2,1:T(8,128)(2,1)S(1)} %bitcast.44, bf16[1536,4,2,64]{0,3,2,1:T(8,128)(2,1)} %bitcast.42), kind=kOutput, calls=%fused_computation.1 | convolution fusion | flops 306706944 | bytes 11212800 | tf_op jit(solution)/shard_map/while/body/eval_jaxpr/qhmd,khmd->hmqk/dot_general | solution.py:37
  70.5 0.0 copy-start.1
  70.5 1.7 %fusion = f32[4,2,192]{2,1,0:T(2,128)S(1)} fusion(f32[4,2,192,1536]{3,2,1,0:T(8,128)S(1)} %get-tuple-element.33, f32[4,2,192]{2,1,0:T(2,128)S(1)} %broadcast_maximum_fusion), kind=kLoop, calls=%fused_computation.2 | loop fusion | flops 7076352 | bytes 9449472 | tf_op jit(solution)/shard_map/while/body/eval_jaxpr/reduce_sum | solution.py:43
  72.3 1.9 %copy-done.1 = f32[4,2,192,1536]{3,2,1,0:T(8,128)} copy-done((f32[4,2,192,1536]{3,2,1,0:T(8,128)}, f32[4,2,192,1536]{3,2,1,0:T(8,128)S(1)}, u32[]{:S(2)}) %copy-start.1) | copy-done | bytes 9437208
  74.2 35.6 %all-gather.5.cloned.1.call-done = bf16[1536,512]{1,0:T(8,128)(2,1)} async-done(((bf16[192,512]{1,0:T(8,128)(2,1)}), bf16[1536,512]{1,0:T(8,128)(2,1)}) %all-gather.5.cloned.1.call-update) | async-done | bytes 1572880 | tf_op jit(solution)/shard_map/all_gather | solution.py:57
  109.8 3.5 %squeeze.17 = bf16[1536,4,128]{2,1,0:T(4,128)(2,1)} reshape(bf16[1536,512]{1,0:T(8,128)(2,1)} %all-gather.5.cloned.1.call-done) | data formatting | bytes 3145728 | tf_op jit(solution)/shard_map/while/body/jit(dynamic_index_in_dim)/squeeze | solution.py:64
  113.3 0.0 copy-start.2
  113.3 0.0 copy-start.3
  113.3 5.4 %fusion.7 = f32[4,2,192,128]{3,2,1,0:T(8,128)S(1)} fusion(bf16[1536,4,128,1]{2,1,0,3:T(4,128)(2,1)} %bitcast.43, f32[4,2,192,1536]{3,2,1,0:T(8,128)} %copy-done.1, f32[4,2,192]{2,1,0:T(2,128)S(1)} %broadcast_maximum_fusion, f32[4,2,192]{2,1,0:T(2,128)S(1)} %get-tuple-element.28), kind=kOutput, calls=%fused_computation.9 | convolution fusion | flops 611254272 | bytes 11808768 | tf_op jit(solution)/shard_map/while/body/eval_jaxpr/hmqk,khe->hmqe/dot_general | solution.py:45
  118.7 0.0 copy-done.2
  118.7 0.5 multiply_reduce_fusion.1
  119.2 0.0 copy-done
  119.2 0.0 copy-done.3
  119.2 1.5 %convolution_convert_fusion = bf16[192,2048]{1,0:T(8,128)(2,1)} fusion(bf16[512,2048]{1,0:T(8,128)(2,1)S(1)} %copy-done, f32[4,192,128]{2,1,0:T(8,128)S(1)} %get-tuple-element.18, f32[128]{0:T(128)S(1)} %copy-done.3, f32[4,192]{1,0:T(4,128)S(1)} %add_rsqrt_fusion), kind=kOutput, calls=%fused_computation.7 | convolution fusion | flops 403341312 | bytes 3280384 | tf_op jit(solution)/shard_map/dot_general | solution.py:74
  120.8 0.0 reduce-scatter.2.cloned.1.call-update
  120.8 21.7 %reduce-scatter.2.cloned.1.call-done = bf16[48,2048]{1,0:T(8,128)(2,1)} async-done(((bf16[192,2048]{1,0:T(8,128)(2,1)}), bf16[48,2048]{1,0:T(8,128)(2,1)}) %reduce-scatter.2.cloned.1.call-update) | async-done | bytes 196624 | tf_op jit(solution)/shard_map/reduce_scatter | solution.py:73
  (5 shorter events, 0.0 us)
Async XLA Ops:
  6.5 112.7 %copy-start = (bf16[512,2048]{1,0:T(8,128)(2,1)S(1)}, bf16[512,2048]{1,0:T(8,128)(2,1)}, u32[]{:S(2)}) copy-start(bf16[512,2048]{1,0:T(8,128)(2,1)} %param.11) | copy-start | bytes 6291460
  6.5 58.5 %all-gather.3.cloned.1.call-start = ((), (), s32[]{:S(2)}) async-start(), calls=%async_computation.1 | async-start | bytes 1769472 | tf_op jit(solution)/shard_map/all_gather | solution.py:56
  19.8 89.9 %all-gather.5.cloned.1.call-start = ((), (), s32[]{:S(2)}) async-start(), calls=%async_computation.2 | async-start | bytes 1769472 | tf_op jit(solution)/shard_map/all_gather | solution.py:57
  22.8 119.8 %reduce-scatter.2.cloned.1.call-start = ((), (), s32[]{:S(2)}) async-start(), calls=%async_computation.3 | async-start | bytes 983040 | tf_op jit(solution)/shard_map/reduce_scatter | solution.py:73
  70.5 3.6 %copy-start.1 = (f32[4,2,192,1536]{3,2,1,0:T(8,128)}, f32[4,2,192,1536]{3,2,1,0:T(8,128)S(1)}, u32[]{:S(2)}) copy-start(f32[4,2,192,1536]{3,2,1,0:T(8,128)S(1)} %get-tuple-element.33) | copy-start | bytes 28311556
  113.3 5.5 %copy-start.2 = (f32[4]{0:T(128)S(1)}, f32[4]{0:T(128)}, u32[]{:S(2)}) copy-start(f32[4]{0:T(128)} %param.12) | copy-start | bytes 52
  113.3 6.0 %copy-start.3 = (f32[128]{0:T(128)S(1)}, f32[128]{0:T(128)}, u32[]{:S(2)}) copy-start(f32[128]{0:T(128)} %param.13) | copy-start | bytes 1540
Sparse Core Ops, SparseCore 0:
  20.0 44.9 all-gather.2
  67.2 42.5 all-gather.4
  120.9 21.5 reduce-scatter.1
where the time goes:
time: 149 us
  waiting for transfers between devices  97.2 us (65%)
  matrix products  17.8 us (12%)
  between operations  13.2 us (9%)
  blocking collectives  10.4 us (7%)
  local copies, waits for them, and re-layouts  8.14 us (5%)
  other arithmetic  2.24 us (2%)
    all_gather x1, waiting for transfers between devices, shards(): lax.all_gather(keys, 'sp', axis=0, tiled=True)  39.9 us
    all_gather x1, waiting for transfers between devices, shards(): lax.all_gather(values, 'sp', axis=0, tiled=True)  35.6 us
    reduce_scatter x1, waiting for transfers between devices, shards(): lax.psum_scatter(jnp.dot(normed, w_out, preferred_element_type=jnp.float3...  21.7 us
    all_gather x1, blocking collectives, shards(): piece = lax.all_gather(tokens, 'tp', axis=0, tiled=True)  10.4 us
    dot_general x1, matrix products, step(): jnp.einsum('hmqk,khe->hmqe', weights, value_blk, preferred_element_type=j...  5.44 us
    squeeze x1, local copies, waits for them, and re-layouts, shards(): carry, unused = lax.scan(step, carry, (key_blocks, value_blocks))  3.51 us
  transfers between devices with their start and end apart: 3, of which 3 were waited for; matrix products, arithmetic and copies ran while one was open for 8% of the time, Pallas kernels for 0%

commit v1 on v0

--- a/solution.py
+++ b/solution.py
@@ -1,6 +1,11 @@
+import functools
+import math
+
 import jax
 import jax.numpy as jnp
 from jax import lax
+from jax.experimental import pallas as pl
+from jax.experimental.pallas import tpu as pltpu
 from jax.sharding import PartitionSpec as P
 
 
@@ -78,6 +83,221 @@
     )
 
 
+BF16 = jnp.bfloat16
+F32 = jnp.float32
+MESH = pl.DeviceIdType.MESH
+CHUNKS = 4
+
+
+def remote(src, dst, send, recv, where):
+    return pltpu.make_async_remote_copy(
+        src_ref=src, dst_ref=dst, send_sem=send, recv_sem=recv, device_id=where, device_id_type=MESH
+    )
+
+
+def kernel(
+    nh, mix_ref, gain_ref, tok_ref, wq_hbm, wk_hbm, wv_hbm, wo_hbm, out_ref,
+    wq, wk, wv, wo, tok, snd, rcv, kvx, nsnd, nrm, keep, dsnd, drcv, ysnd, yrcv,
+    w_sem, a_ss, a_rs, z_ss, z_rs, x_ss, x_rs, c_ss, c_rs, d_ss, d_rs, y_ss, y_rs,
+):
+    rows, width = tok_ref.shape
+    pair = 2 * rows
+    block = 2 * pair
+    vd = gain_ref.shape[1]
+    s, t = lax.axis_index("sp"), lax.axis_index("tp")
+    h, g = s // 2, s % 2
+    core_peer = {"tp": t + 1 - 2 * (t % 2)}
+    row_peer = {"tp": t + 2 - 4 * (t // 2)}
+    side_peer = {"sp": h * 2 + (1 - g)}
+
+    def head_peer(d):
+        return {"sp": lax.rem(h + d, nh) * 2 + g}
+
+    loads = [
+        pltpu.make_async_copy(a, b, w_sem.at[i])
+        for i, (a, b) in enumerate(((wq_hbm, wq), (wk_hbm, wk), (wv_hbm, wv), (wo_hbm, wo)))
+    ]
+    for load in loads:
+        load.start()
+
+    barrier = pltpu.get_barrier_semaphore()
+    peers = [core_peer, row_peer, side_peer] + [head_peer(d) for d in range(1, nh)]
+    for peer in peers:
+        pl.semaphore_signal(barrier, inc=1, device_id=peer, device_id_type=MESH)
+    pl.semaphore_wait(barrier, len(peers))
+
+    pending = []
+    to_row = remote(tok_ref, tok.at[1], a_ss.at[1], a_rs.at[1], row_peer)
+    to_row.start()
+    to_core = remote(tok_ref, tok.at[0], a_ss.at[0], a_rs.at[0], core_peer)
+    to_core.start()
+    forward = remote(tok.at[1], tok.at[2], a_ss.at[2], a_rs.at[2], core_peer)
+    pending += [to_row, to_core, forward]
+
+    z_copies, x_copies = {}, {}
+
+    def project(p, x):
+        at = pl.ds(p * pair, pair)
+        for i, w in enumerate((wq, wk, wv)):
+            if p == 0:
+                loads[i].wait()
+            y = jnp.dot(x, w[...], preferred_element_type=F32).astype(BF16)
+            for hh in range(nh):
+                snd[hh, i, at, :] = y[:, hh * vd : (hh + 1) * vd]
+        for d in range(1, nh):
+            z_copies[p, d] = remote(
+                snd.at[lax.rem(h + d, nh), :, at, :],
+                rcv.at[:, pl.ds(d * block + p * pair, pair), :],
+                z_ss.at[p, d - 1],
+                z_rs.at[p, d - 1],
+                head_peer(d),
+            )
+            z_copies[p, d].start()
+        x_copies[p, 0] = remote(
+            snd.at[h, pl.ds(1, 2), at, :], kvx.at[:, at, :], x_ss.at[p, 0], x_rs.at[p, 0], side_peer
+        )
+        x_copies[p, 0].start()
+        rcv[:, at, :] = snd[h, :, at, :]
+
+    def relay(p, d):
+        z_copies[p, d].wait_recv()
+        at = pl.ds(d * block + p * pair, pair)
+        x_copies[p, d] = remote(
+            rcv.at[pl.ds(1, 2), at, :], kvx.at[:, at, :], x_ss.at[p, d], x_rs.at[p, d], side_peer
+        )
+        x_copies[p, d].start()
+
+    to_core.wait_recv()
+    project(0, jnp.concatenate([tok_ref[...], tok[0]], axis=0))
+    to_row.wait_recv()
+    forward.start()
+    forward.wait_recv()
+    project(1, tok[1:3].reshape(pair, width))
+    for p in range(2):
+        for d in range(1, nh):
+            relay(p, d)
+    for p in range(2):
+        for d in range(nh):
+            x_copies[p, d].wait_recv()
+
+    pending += list(z_copies.values()) + list(x_copies.values())
+
+    hd = vd // 2
+    c = (hd ** -0.5) * math.log2(math.e)
+    lam = mix_ref[h]
+    gain = gain_ref[...]
+    lane = lax.broadcasted_iota(jnp.int32, (block, vd), 1)
+    c_copies = []
+    nt = (((1,), (1,)), ((), ()))
+    for d in list(range(1, nh)) + [0]:
+        q = rcv[0, pl.ds(d * block, block), :]
+        zero = jnp.zeros_like(q)
+        qq = jnp.concatenate([jnp.where(lane < hd, q, zero), jnp.where(lane < hd, zero, q)], axis=0)
+        s0 = lax.dot_general(qq, rcv[1], nt, preferred_element_type=F32)
+        s1 = lax.dot_general(qq, kvx[0], nt, preferred_element_type=F32)
+        top = jnp.maximum(jnp.max(s0, axis=1, keepdims=True), jnp.max(s1, axis=1, keepdims=True))
+        e0 = jnp.exp2((s0 - top) * c)
+        e1 = jnp.exp2((s1 - top) * c)
+        total = jnp.sum(e0, axis=1, keepdims=True) + jnp.sum(e1, axis=1, keepdims=True)
+        acc = jnp.dot(e0.astype(BF16), rcv[2], preferred_element_type=F32)
+        acc = acc + jnp.dot(e1.astype(BF16), kvx[1], preferred_element_type=F32)
+        o = acc / total
+        o = o[:block] - lam * o[block:]
+        meansq = jnp.mean(o * o, axis=1, keepdims=True)
+        normed = (o * lax.rsqrt(meansq + 1e-06) * gain).astype(BF16)
+        if d == 0:
+            nrm[h] = normed
+        else:
+            nsnd[d - 1] = normed
+            back = remote(
+                nsnd.at[d - 1], nrm.at[h], c_ss.at[d - 1], c_rs.at[d - 1], head_peer(nh - d)
+            )
+            back.start()
+            c_copies.append(back)
+    for back in c_copies:
+        back.wait_recv()
+    pending += c_copies
+
+    loads[3].wait()
+    n = jnp.concatenate([nrm[i] for i in range(nh)], axis=1)
+    step = width // CHUNKS
+    d_copies, y_copies = [], []
+    for k in range(CHUNKS):
+        part = jnp.dot(n, wo[:, k * step : (k + 1) * step], preferred_element_type=F32)
+        dsnd[k, 0] = part[rows : 2 * rows].astype(BF16)
+        dsnd[k, 1] = part[3 * rows :].astype(BF16)
+        keep[0, k] = part[:rows]
+        keep[1, k] = part[2 * rows : 3 * rows]
+        d_copies.append(remote(dsnd.at[k], drcv.at[k], d_ss.at[k], d_rs.at[k], core_peer))
+        d_copies[k].start()
+        y_copies.append(remote(ysnd.at[k], yrcv.at[k], y_ss.at[k], y_rs.at[k], row_peer))
+    for k in range(CHUNKS):
+        d_copies[k].wait_recv()
+        ysnd[k] = (keep[1, k] + drcv[k, 1].astype(F32)).astype(BF16)
+        y_copies[k].start()
+    for k in range(CHUNKS):
+        y_copies[k].wait_recv()
+        whole = keep[0, k] + drcv[k, 0].astype(F32) + yrcv[k].astype(F32)
+        out_ref[:, k * step : (k + 1) * step] = whole.astype(BF16)
+    for copy in pending + d_copies + y_copies:
+        copy.wait_send()
+
+
+def fused(tokens, w_query, w_key, w_value, w_out, mix_weight, out_gain):
+    rows, width = tokens.shape
+    nh = mix_weight.shape[0]
+    vd = out_gain.shape[0]
+    cols = w_query.shape[1]
+    block = 4 * rows
+    step = width // CHUNKS
+    vmem, hbm = pl.BlockSpec(memory_space=pltpu.VMEM), pl.BlockSpec(memory_space=pl.ANY)
+    dma = pltpu.SemaphoreType.DMA
+    return pl.pallas_call(
+        functools.partial(kernel, nh),
+        out_shape=jax.ShapeDtypeStruct((rows, width), BF16),
+        in_specs=[pl.BlockSpec(memory_space=pltpu.SMEM), vmem, vmem, hbm, hbm, hbm, hbm],
+        out_specs=vmem,
+        scratch_shapes=[
+            pltpu.VMEM((width, cols), BF16),
+            pltpu.VMEM((width, cols), BF16),
+            pltpu.VMEM((width, cols), BF16),
+            pltpu.VMEM(w_out.shape, BF16),
+            pltpu.VMEM((3, rows, width), BF16),
+            pltpu.VMEM((nh, 3, block, vd), BF16),
+            pltpu.VMEM((3, nh * block, vd), BF16),
+            pltpu.VMEM((2, nh * block, vd), BF16),
+            pltpu.VMEM((nh - 1, block, vd), BF16),
+            pltpu.VMEM((nh, block, vd), BF16),
+            pltpu.VMEM((2, CHUNKS, rows, step), F32),
+            pltpu.VMEM((CHUNKS, 2, rows, step), BF16),
+            pltpu.VMEM((CHUNKS, 2, rows, step), BF16),
+            pltpu.VMEM((CHUNKS, rows, step), BF16),
+            pltpu.VMEM((CHUNKS, rows, step), BF16),
+            dma((4,)), dma((3,)), dma((3,)),
+            dma((2, nh - 1)), dma((2, nh - 1)), dma((2, nh)), dma((2, nh)),
+            dma((nh - 1,)), dma((nh - 1,)),
+            dma((CHUNKS,)), dma((CHUNKS,)), dma((CHUNKS,)), dma((CHUNKS,)),
+        ],
+        compiler_params=pltpu.CompilerParams(
+            collective_id=0, has_side_effects=True, vmem_limit_bytes=56 * 2**20
+        ),
+    )(mix_weight, out_gain.reshape(1, vd), tokens, w_query, w_key, w_value, w_out)
+
+
+def pick(mesh, *arrays):
+    tokens, w_query, _, _, _, mix_weight, out_gain = arrays
+    nh = mix_weight.shape[0]
+    fits = (
+        mesh.shape["sp"] == 2 * nh
+        and mesh.shape["tp"] == 4
+        and w_query.shape[1] == nh * out_gain.shape[0]
+        and out_gain.shape[0] == 128
+        and tokens.shape[0] % 16 == 0
+        and tokens.shape[1] % (128 * CHUNKS) == 0
+    )
+    return fused(*arrays) if fits else shards(*arrays)
+
+
 def solution(mesh):
     in_specs = (
         P(("sp", "tp"), None),
@@ -89,4 +309,4 @@
         P(),
     )
     out_specs = P(("sp", "tp"), None)
-    return jax.shard_map(shards, mesh=mesh, in_specs=in_specs, out_specs=out_specs, check_vma=False)
+    return jax.shard_map(functools.partial(pick, mesh), mesh=mesh, in_specs=in_specs, out_specs=out_specs, check_vma=False)

time: 149 us -> 47.7 us (0.32)
  waiting for transfers between devices: 97.2 us -> 0 us
  Pallas kernels: 0 us -> 46 us
  matrix products: 17.8 us -> 0 us
  between operations: 13.2 us -> 0.01 us
  blocking collectives: 10.4 us -> 0 us
  local copies, waits for them, and re-layouts: 8.14 us -> 1.62 us
  other arithmetic: 2.24 us -> 0 us
    all_gather x2 -> x0, waiting for transfers between devices: 75.4 us -> none  [the longest x1 39.9 us: shards(): lax.all_gather(keys, 'sp', axis=0, tiled=True)]
    pallas_call x0 -> x1, Pallas kernels: none -> 46 us  [fused(): pl.pallas_call(functools.partial(kernel, nh), out_shape=jax.ShapeDtypeStr...]
    reduce_scatter x1 -> x0, waiting for transfers between devices: 21.7 us -> none  [shards(): lax.psum_scatter(jnp.dot(normed, w_out, preferred_element_type=jnp.float3...]
    dot_general x6 -> x0, matrix products: 17.8 us -> none  [the longest x1 5.44 us: step(): jnp.einsum('hmqk,khe->hmqe', weights, value_blk, preferred_element_type=j...]
    all_gather x1 -> x0, blocking collectives: 10.4 us -> none  [shards(): piece = lax.all_gather(tokens, 'tp', axis=0, tiled=True)]
    squeeze x1 -> x0, local copies, waits for them, and re-layouts: 3.51 us -> none  [shards(): carry, unused = lax.scan(step, carry, (key_blocks, value_blocks))]
    all_gather x1 -> x0, local copies, waits for them, and re-layouts: 2.59 us -> none  [shards(): lax.all_gather(keys, 'sp', axis=0, tiled=True)]
    reduce_sum x2 -> x0, other arithmetic: 2.21 us -> none  [the longest x1 1.73 us: step(): running_sum = running_sum * factor + jnp.sum(expw, axis=-1)]
  transfers between devices with their start and end apart: 3 -> 0, of which waited for: 3 -> 0; matrix products, arithmetic and copies ran while one was open for 8% -> 0% of each run, Pallas kernels for 0% -> 0%
where the time goes in v1:
time: 47.7 us; the launch traced here: 47.6 us
  Pallas kernels  46 us (96%)
  local copies, waits for them, and re-layouts  1.62 us (3%)
    pallas_call x1, Pallas kernels, fused(): pl.pallas_call(functools.partial(kernel, nh), out_shape=jax.ShapeDtypeStr...  46 us
    unnamed x1, local copies, waits for them, and re-layouts  1.62 us

profile of v1, /device:TPU:0, one launch (start us, length us, event | category | flops | bytes accessed | tf_op | source)
XLA Modules:
  0.0 47.6 jit_solution(12423977344296571137)
XLA Ops:
  0.0 46.0 %shard_map.73 = bf16[48,2048]{1,0:T(8,128)(2,1)} custom-call(f32[4]{0:T(128)} %mix_ref.1, f32[1,128]{1,0:T(1,128)} %bitcast.1, bf16[48,2048]{1,0:T(8,128)(2,1)} %tok_ref.1, bf16[2048,512]{1,0:T(8,128)(2,1)} %wq_hbm.1, bf16[2048,512]{1,0:T(8,128)(2,1)} %wk_hbm.1, bf16[2048,512]{1,0:T(8,128)(2,1)} %wv_hbm.1, bf16[512,2048]{1,0:T(8,128)(2,1)} %wo_hbm.1), custom_call_target="tpu_custom_call" | custom-call | tf_op jit(solution)/shard_map/pallas_call | solution.py:255
  46.0 1.6 %copy.9 = bf16[48,2048]{1,0:T(8,128)(2,1)} copy(bf16[48,2048]{1,0:T(8,128)(2,1)} %shard_map.73) | data formatting | bytes 393216

commit v2 on v1

--- a/solution.py
+++ b/solution.py
@@ -102,7 +102,6 @@
 ):
     rows, width = tok_ref.shape
     pair = 2 * rows
-    block = 2 * pair
     vd = gain_ref.shape[1]
     s, t = lax.axis_index("sp"), lax.axis_index("tp")
     h, g = s // 2, s % 2
@@ -134,38 +133,95 @@
     forward = remote(tok.at[1], tok.at[2], a_ss.at[2], a_rs.at[2], core_peer)
     pending += [to_row, to_core, forward]
 
-    z_copies, x_copies = {}, {}
+    half = nh * pair
+    z_copies, q_copies, x_copies = {}, {}, {}
+
+    def at(p, d):
+        return pl.ds(p * half + d * pair, pair)
 
     def project(p, x):
-        at = pl.ds(p * pair, pair)
+        mine = pl.ds(p * pair, pair)
         for i, w in enumerate((wq, wk, wv)):
             if p == 0:
                 loads[i].wait()
             y = jnp.dot(x, w[...], preferred_element_type=F32).astype(BF16)
             for hh in range(nh):
-                snd[hh, i, at, :] = y[:, hh * vd : (hh + 1) * vd]
-        for d in range(1, nh):
-            z_copies[p, d] = remote(
-                snd.at[lax.rem(h + d, nh), :, at, :],
-                rcv.at[:, pl.ds(d * block + p * pair, pair), :],
-                z_ss.at[p, d - 1],
-                z_rs.at[p, d - 1],
-                head_peer(d),
-            )
-            z_copies[p, d].start()
+                snd[hh, i, mine, :] = y[:, hh * vd : (hh + 1) * vd]
         x_copies[p, 0] = remote(
-            snd.at[h, pl.ds(1, 2), at, :], kvx.at[:, at, :], x_ss.at[p, 0], x_rs.at[p, 0], side_peer
+            snd.at[h, pl.ds(1, 2), mine, :], kvx.at[:, at(p, 0), :], x_ss.at[p, 0], x_rs.at[p, 0], side_peer
         )
         x_copies[p, 0].start()
-        rcv[:, at, :] = snd[h, :, at, :]
-
-    def relay(p, d):
-        z_copies[p, d].wait_recv()
-        at = pl.ds(d * block + p * pair, pair)
-        x_copies[p, d] = remote(
-            rcv.at[pl.ds(1, 2), at, :], kvx.at[:, at, :], x_ss.at[p, d], x_rs.at[p, d], side_peer
-        )
-        x_copies[p, d].start()
+        for copies, i, n, sem in ((z_copies, 1, 2, 0), (q_copies, 0, 1, 1)):
+            for d in range(1, nh):
+                copies[p, d] = remote(
+                    snd.at[lax.rem(h + d, nh), pl.ds(i, n), mine, :],
+                    rcv.at[pl.ds(i, n), at(p, d), :],
+                    z_ss.at[sem, p, d - 1],
+                    z_rs.at[sem, p, d - 1],
+                    head_peer(d),
+                )
+                copies[p, d].start()
+        rcv[:, at(p, 0), :] = snd[h, :, mine, :]
+
+    def relay(p):
+        for d in range(1, nh):
+            z_copies[p, d].wait_recv()
+            x_copies[p, d] = remote(
+                rcv.at[pl.ds(1, 2), at(p, d), :], kvx.at[:, at(p, d), :], x_ss.at[p, d], x_rs.at[p, d], side_peer
+            )
+            x_copies[p, d].start()
+
+    hd = vd // 2
+    c = (hd ** -0.5) * math.log2(math.e)
+    lam = mix_ref[h]
+    gain = gain_ref[...]
+    lane = lax.broadcasted_iota(jnp.int32, (half, vd), 1)
+    nt = (((1,), (1,)), ((), ()))
+    state = {}
+
+    def attend(p, k, v):
+        q = rcv[0, pl.ds(p * half, half), :]
+        zero = jnp.zeros_like(q)
+        qq = jnp.concatenate([jnp.where(lane < hd, q, zero), jnp.where(lane < hd, zero, q)], axis=0)
+        scores = lax.dot_general(qq, k, nt, preferred_element_type=F32)
+        top = jnp.max(scores, axis=1, keepdims=True)
+        if p in state:
+            top = jnp.maximum(top, state[p][0])
+        expw = jnp.exp2((scores - top) * c)
+        total = jnp.sum(expw, axis=1, keepdims=True)
+        acc = jnp.dot(expw.astype(BF16), v, preferred_element_type=F32)
+        if p in state:
+            factor = jnp.exp2((state[p][0] - top) * c)
+            total = total + state[p][1] * factor
+            acc = acc + state[p][2] * factor
+        state[p] = (top, total, acc)
+
+    def own(p, kp):
+        attend(p, rcv[1, pl.ds(kp * half, half), :], rcv[2, pl.ds(kp * half, half), :])
+
+    def side(p, kp):
+        attend(p, kvx[0, pl.ds(kp * half, half), :], kvx[1, pl.ds(kp * half, half), :])
+
+    c_copies = {}
+
+    def finish(p):
+        _, total, acc = state[p]
+        o = acc / total
+        o = o[:half] - lam * o[half:]
+        meansq = jnp.mean(o * o, axis=1, keepdims=True)
+        normed = (o * lax.rsqrt(meansq + 1e-06) * gain).astype(BF16)
+        for d in range(1, nh):
+            nsnd[p, d - 1] = normed[d * pair : (d + 1) * pair]
+            c_copies[p, d] = remote(
+                nsnd.at[p, d - 1], nrm.at[p, h], c_ss.at[p, d - 1], c_rs.at[p, d - 1], head_peer(nh - d)
+            )
+            c_copies[p, d].start()
+        nrm[p, h] = normed[:pair]
+
+    def arrived(copies, p):
+        for (cp, d), copy in copies.items():
+            if cp == p:
+                copy.wait_recv()
 
     to_core.wait_recv()
     project(0, jnp.concatenate([tok_ref[...], tok[0]], axis=0))
@@ -173,73 +229,52 @@
     forward.start()
     forward.wait_recv()
     project(1, tok[1:3].reshape(pair, width))
-    for p in range(2):
-        for d in range(1, nh):
-            relay(p, d)
-    for p in range(2):
-        for d in range(nh):
-            x_copies[p, d].wait_recv()
-
-    pending += list(z_copies.values()) + list(x_copies.values())
-
-    hd = vd // 2
-    c = (hd ** -0.5) * math.log2(math.e)
-    lam = mix_ref[h]
-    gain = gain_ref[...]
-    lane = lax.broadcasted_iota(jnp.int32, (block, vd), 1)
-    c_copies = []
-    nt = (((1,), (1,)), ((), ()))
-    for d in list(range(1, nh)) + [0]:
-        q = rcv[0, pl.ds(d * block, block), :]
-        zero = jnp.zeros_like(q)
-        qq = jnp.concatenate([jnp.where(lane < hd, q, zero), jnp.where(lane < hd, zero, q)], axis=0)
-        s0 = lax.dot_general(qq, rcv[1], nt, preferred_element_type=F32)
-        s1 = lax.dot_general(qq, kvx[0], nt, preferred_element_type=F32)
-        top = jnp.maximum(jnp.max(s0, axis=1, keepdims=True), jnp.max(s1, axis=1, keepdims=True))
-        e0 = jnp.exp2((s0 - top) * c)
-        e1 = jnp.exp2((s1 - top) * c)
-        total = jnp.sum(e0, axis=1, keepdims=True) + jnp.sum(e1, axis=1, keepdims=True)
-        acc = jnp.dot(e0.astype(BF16), rcv[2], preferred_element_type=F32)
-        acc = acc + jnp.dot(e1.astype(BF16), kvx[1], preferred_element_type=F32)
-        o = acc / total
-        o = o[:block] - lam * o[block:]
-        meansq = jnp.mean(o * o, axis=1, keepdims=True)
-        normed = (o * lax.rsqrt(meansq + 1e-06) * gain).astype(BF16)
-        if d == 0:
-            nrm[h] = normed
-        else:
-            nsnd[d - 1] = normed
-            back = remote(
-                nsnd.at[d - 1], nrm.at[h], c_ss.at[d - 1], c_rs.at[d - 1], head_peer(nh - d)
-            )
-            back.start()
-            c_copies.append(back)
-    for back in c_copies:
-        back.wait_recv()
-    pending += c_copies
+    relay(0)
+    arrived(q_copies, 0)
+    own(0, 0)
+    arrived(x_copies, 0)
+    side(0, 0)
+    relay(1)
+    own(0, 1)
+    arrived(q_copies, 1)
+    own(1, 0)
+    side(1, 0)
+    own(1, 1)
+    arrived(x_copies, 1)
+    side(1, 1)
+    finish(1)
+    side(0, 1)
+    finish(0)
+
+    step = width // CHUNKS
+    d_copies, y_copies = {}, []
+
+    def out_part(p):
+        arrived(c_copies, p)
+        n = jnp.concatenate([nrm[p, i] for i in range(nh)], axis=1)
+        for k in range(CHUNKS):
+            part = jnp.dot(n, wo[:, k * step : (k + 1) * step], preferred_element_type=F32)
+            dsnd[p, k] = part[rows:].astype(BF16)
+            keep[p, k] = part[:rows]
+            d_copies[p, k] = remote(dsnd.at[p, k], drcv.at[p, k], d_ss.at[p, k], d_rs.at[p, k], core_peer)
+            d_copies[p, k].start()
 
     loads[3].wait()
-    n = jnp.concatenate([nrm[i] for i in range(nh)], axis=1)
-    step = width // CHUNKS
-    d_copies, y_copies = [], []
+    out_part(1)
     for k in range(CHUNKS):
-        part = jnp.dot(n, wo[:, k * step : (k + 1) * step], preferred_element_type=F32)
-        dsnd[k, 0] = part[rows : 2 * rows].astype(BF16)
-        dsnd[k, 1] = part[3 * rows :].astype(BF16)
-        keep[0, k] = part[:rows]
-        keep[1, k] = part[2 * rows : 3 * rows]
-        d_copies.append(remote(dsnd.at[k], drcv.at[k], d_ss.at[k], d_rs.at[k], core_peer))
-        d_copies[k].start()
+        d_copies[1, k].wait_recv()
+        ysnd[k] = (keep[1, k] + drcv[1, k].astype(F32)).astype(BF16)
         y_copies.append(remote(ysnd.at[k], yrcv.at[k], y_ss.at[k], y_rs.at[k], row_peer))
+        y_copies[k].start()
+    out_part(0)
     for k in range(CHUNKS):
-        d_copies[k].wait_recv()
-        ysnd[k] = (keep[1, k] + drcv[k, 1].astype(F32)).astype(BF16)
-        y_copies[k].start()
-    for k in range(CHUNKS):
+        d_copies[0, k].wait_recv()
         y_copies[k].wait_recv()
-        whole = keep[0, k] + drcv[k, 0].astype(F32) + yrcv[k].astype(F32)
+        whole = keep[0, k] + drcv[0, k].astype(F32) + yrcv[k].astype(F32)
         out_ref[:, k * step : (k + 1) * step] = whole.astype(BF16)
-    for copy in pending + d_copies + y_copies:
+    for copies in (z_copies, q_copies, x_copies, c_copies, d_copies):
+        pending += list(copies.values())
+    for copy in pending + y_copies:
         copy.wait_send()
 
 
@@ -266,17 +301,17 @@
             pltpu.VMEM((nh, 3, block, vd), BF16),
             pltpu.VMEM((3, nh * block, vd), BF16),
             pltpu.VMEM((2, nh * block, vd), BF16),
-            pltpu.VMEM((nh - 1, block, vd), BF16),
-            pltpu.VMEM((nh, block, vd), BF16),
+            pltpu.VMEM((2, nh - 1, 2 * rows, vd), BF16),
+            pltpu.VMEM((2, nh, 2 * rows, vd), BF16),
             pltpu.VMEM((2, CHUNKS, rows, step), F32),
-            pltpu.VMEM((CHUNKS, 2, rows, step), BF16),
-            pltpu.VMEM((CHUNKS, 2, rows, step), BF16),
+            pltpu.VMEM((2, CHUNKS, rows, step), BF16),
+            pltpu.VMEM((2, CHUNKS, rows, step), BF16),
             pltpu.VMEM((CHUNKS, rows, step), BF16),
             pltpu.VMEM((CHUNKS, rows, step), BF16),
             dma((4,)), dma((3,)), dma((3,)),
-            dma((2, nh - 1)), dma((2, nh - 1)), dma((2, nh)), dma((2, nh)),
-            dma((nh - 1,)), dma((nh - 1,)),
-            dma((CHUNKS,)), dma((CHUNKS,)), dma((CHUNKS,)), dma((CHUNKS,)),
+            dma((2, 2, nh - 1)), dma((2, 2, nh - 1)), dma((2, nh)), dma((2, nh)),
+            dma((2, nh - 1)), dma((2, nh - 1)),
+            dma((2, CHUNKS)), dma((2, CHUNKS)), dma((CHUNKS,)), dma((CHUNKS,)),
         ],
         compiler_params=pltpu.CompilerParams(
             collective_id=0, has_side_effects=True, vmem_limit_bytes=56 * 2**20

time: 47.7 us -> 43.6 us (0.914)
  Pallas kernels: 46 us -> 41.8 us
    pallas_call x1, Pallas kernels: 46 us -> 41.8 us  [fused(): pl.pallas_call(functools.partial(kernel, nh), out_shape=jax.ShapeDtypeStr...]
where the time goes in v2:
time: 43.6 us; the launch traced here: 43.4 us
  Pallas kernels  41.8 us (96%)
  local copies, waits for them, and re-layouts  1.62 us (4%)
    pallas_call x1, Pallas kernels, fused(): pl.pallas_call(functools.partial(kernel, nh), out_shape=jax.ShapeDtypeStr...  41.8 us
    unnamed x1, local copies, waits for them, and re-layouts  1.62 us

profile of v2, /device:TPU:0, one launch (start us, length us, event | category | flops | bytes accessed | tf_op | source)
XLA Modules:
  0.0 43.4 jit_solution(13253303591271907398)
XLA Ops:
  0.0 41.8 %shard_map.73 = bf16[48,2048]{1,0:T(8,128)(2,1)} custom-call(f32[4]{0:T(128)} %mix_ref.1, f32[1,128]{1,0:T(1,128)} %bitcast.1, bf16[48,2048]{1,0:T(8,128)(2,1)} %tok_ref.1, bf16[2048,512]{1,0:T(8,128)(2,1)} %wq_hbm.1, bf16[2048,512]{1,0:T(8,128)(2,1)} %wk_hbm.1, bf16[2048,512]{1,0:T(8,128)(2,1)} %wv_hbm.1, bf16[512,2048]{1,0:T(8,128)(2,1)} %wo_hbm.1), custom_call_target="tpu_custom_call" | custom-call | tf_op jit(solution)/shard_map/pallas_call | solution.py:290
  41.8 1.6 %copy.9 = bf16[48,2048]{1,0:T(8,128)(2,1)} copy(bf16[48,2048]{1,0:T(8,128)(2,1)} %shard_map.73) | data formatting | bytes 393216

commit v3 on v2

--- a/solution.py
+++ b/solution.py
@@ -123,53 +123,49 @@
     peers = [core_peer, row_peer, side_peer] + [head_peer(d) for d in range(1, nh)]
     for peer in peers:
         pl.semaphore_signal(barrier, inc=1, device_id=peer, device_id_type=MESH)
-    pl.semaphore_wait(barrier, len(peers))
 
     pending = []
-    to_row = remote(tok_ref, tok.at[1], a_ss.at[1], a_rs.at[1], row_peer)
-    to_row.start()
-    to_core = remote(tok_ref, tok.at[0], a_ss.at[0], a_rs.at[0], core_peer)
-    to_core.start()
-    forward = remote(tok.at[1], tok.at[2], a_ss.at[2], a_rs.at[2], core_peer)
-    pending += [to_row, to_core, forward]
-
     half = nh * pair
     z_copies, q_copies, x_copies = {}, {}, {}
 
-    def at(p, d):
-        return pl.ds(p * half + d * pair, pair)
-
-    def project(p, x):
-        mine = pl.ds(p * pair, pair)
-        for i, w in enumerate((wq, wk, wv)):
-            if p == 0:
+    quarter = nh * rows
+
+    def at(u, d):
+        return pl.ds(u * quarter + d * rows, rows)
+
+    def project(u, x):
+        for i, w in ((1, wk), (2, wv), (0, wq)):
+            if u == 0:
                 loads[i].wait()
             y = jnp.dot(x, w[...], preferred_element_type=F32).astype(BF16)
             for hh in range(nh):
-                snd[hh, i, mine, :] = y[:, hh * vd : (hh + 1) * vd]
-        x_copies[p, 0] = remote(
-            snd.at[h, pl.ds(1, 2), mine, :], kvx.at[:, at(p, 0), :], x_ss.at[p, 0], x_rs.at[p, 0], side_peer
-        )
-        x_copies[p, 0].start()
+                snd[hh, i, pl.ds(u * rows, rows), :] = y[:, hh * vd : (hh + 1) * vd]
+        rcv[:, at(u, 0), :] = snd[h, :, pl.ds(u * rows, rows), :]
+
+    def send(u):
+        mine = pl.ds(u * rows, rows)
         for copies, i, n, sem in ((z_copies, 1, 2, 0), (q_copies, 0, 1, 1)):
             for d in range(1, nh):
-                copies[p, d] = remote(
+                copies[u, d] = remote(
                     snd.at[lax.rem(h + d, nh), pl.ds(i, n), mine, :],
-                    rcv.at[pl.ds(i, n), at(p, d), :],
-                    z_ss.at[sem, p, d - 1],
-                    z_rs.at[sem, p, d - 1],
+                    rcv.at[pl.ds(i, n), at(u, d), :],
+                    z_ss.at[sem, u, d - 1],
+                    z_rs.at[sem, u, d - 1],
                     head_peer(d),
                 )
-                copies[p, d].start()
-        rcv[:, at(p, 0), :] = snd[h, :, mine, :]
-
-    def relay(p):
+                copies[u, d].start()
+        x_copies[u, 0] = remote(
+            snd.at[h, pl.ds(1, 2), mine, :], kvx.at[:, at(u, 0), :], x_ss.at[u, 0], x_rs.at[u, 0], side_peer
+        )
+        x_copies[u, 0].start()
+
+    def relay(u):
         for d in range(1, nh):
-            z_copies[p, d].wait_recv()
-            x_copies[p, d] = remote(
-                rcv.at[pl.ds(1, 2), at(p, d), :], kvx.at[:, at(p, d), :], x_ss.at[p, d], x_rs.at[p, d], side_peer
+            z_copies[u, d].wait_recv()
+            x_copies[u, d] = remote(
+                rcv.at[pl.ds(1, 2), at(u, d), :], kvx.at[:, at(u, d), :], x_ss.at[u, d], x_rs.at[u, d], side_peer
             )
-            x_copies[p, d].start()
+            x_copies[u, d].start()
 
     hd = vd // 2
     c = (hd ** -0.5) * math.log2(math.e)
@@ -210,37 +206,57 @@
         o = o[:half] - lam * o[half:]
         meansq = jnp.mean(o * o, axis=1, keepdims=True)
         normed = (o * lax.rsqrt(meansq + 1e-06) * gain).astype(BF16)
+        normed = normed.reshape(2, nh, rows, vd)
         for d in range(1, nh):
-            nsnd[p, d - 1] = normed[d * pair : (d + 1) * pair]
+            nsnd[p, d - 1] = normed[:, d]
             c_copies[p, d] = remote(
                 nsnd.at[p, d - 1], nrm.at[p, h], c_ss.at[p, d - 1], c_rs.at[p, d - 1], head_peer(nh - d)
             )
             c_copies[p, d].start()
-        nrm[p, h] = normed[:pair]
+        nrm[p, h] = normed[:, 0]
 
     def arrived(copies, p):
         for (cp, d), copy in copies.items():
             if cp == p:
                 copy.wait_recv()
 
+    project(0, tok_ref[...])
+    pl.semaphore_wait(barrier, len(peers))
+    to_row = remote(tok_ref, tok.at[1], a_ss.at[1], a_rs.at[1], row_peer)
+    to_row.start()
+    to_core = remote(tok_ref, tok.at[0], a_ss.at[0], a_rs.at[0], core_peer)
+    to_core.start()
+    forward = remote(tok.at[1], tok.at[2], a_ss.at[2], a_rs.at[2], core_peer)
+    pending += [to_row, to_core, forward]
+    send(0)
     to_core.wait_recv()
-    project(0, jnp.concatenate([tok_ref[...], tok[0]], axis=0))
+    project(1, tok[0])
+    send(1)
     to_row.wait_recv()
     forward.start()
+    project(2, tok[1])
+    send(2)
     forward.wait_recv()
-    project(1, tok[1:3].reshape(pair, width))
+    project(3, tok[2])
+    send(3)
     relay(0)
-    arrived(q_copies, 0)
+    relay(1)
+    for u in range(2):
+        arrived(q_copies, u)
     own(0, 0)
-    arrived(x_copies, 0)
+    relay(2)
+    for u in range(2):
+        arrived(x_copies, u)
     side(0, 0)
-    relay(1)
+    relay(3)
     own(0, 1)
-    arrived(q_copies, 1)
+    for u in range(2, 4):
+        arrived(q_copies, u)
     own(1, 0)
     side(1, 0)
     own(1, 1)
-    arrived(x_copies, 1)
+    for u in range(2, 4):
+        arrived(x_copies, u)
     side(1, 1)
     finish(1)
     side(0, 1)
@@ -251,7 +267,7 @@
 
     def out_part(p):
         arrived(c_copies, p)
-        n = jnp.concatenate([nrm[p, i] for i in range(nh)], axis=1)
+        n = jnp.concatenate([nrm[p, i].reshape(pair, vd) for i in range(nh)], axis=1)
         for k in range(CHUNKS):
             part = jnp.dot(n, wo[:, k * step : (k + 1) * step], preferred_element_type=F32)
             dsnd[p, k] = part[rows:].astype(BF16)
@@ -301,15 +317,15 @@
             pltpu.VMEM((nh, 3, block, vd), BF16),
             pltpu.VMEM((3, nh * block, vd), BF16),
             pltpu.VMEM((2, nh * block, vd), BF16),
-            pltpu.VMEM((2, nh - 1, 2 * rows, vd), BF16),
-            pltpu.VMEM((2, nh, 2 * rows, vd), BF16),
+            pltpu.VMEM((2, nh - 1, 2, rows, vd), BF16),
+            pltpu.VMEM((2, nh, 2, rows, vd), BF16),
             pltpu.VMEM((2, CHUNKS, rows, step), F32),
             pltpu.VMEM((2, CHUNKS, rows, step), BF16),
             pltpu.VMEM((2, CHUNKS, rows, step), BF16),
             pltpu.VMEM((CHUNKS, rows, step), BF16),
             pltpu.VMEM((CHUNKS, rows, step), BF16),
             dma((4,)), dma((3,)), dma((3,)),
-            dma((2, 2, nh - 1)), dma((2, 2, nh - 1)), dma((2, nh)), dma((2, nh)),
+            dma((2, 4, nh - 1)), dma((2, 4, nh - 1)), dma((4, nh)), dma((4, nh)),
             dma((2, nh - 1)), dma((2, nh - 1)),
             dma((2, CHUNKS)), dma((2, CHUNKS)), dma((CHUNKS,)), dma((CHUNKS,)),
         ],

time: 43.6 us -> 42.7 us (0.979)
  Pallas kernels: 41.8 us -> 41 us
    pallas_call x1, Pallas kernels: 41.8 us -> 41 us  [fused(): pl.pallas_call(functools.partial(kernel, nh), out_shape=jax.ShapeDtypeStr...]
where the time goes in v3:
time: 42.7 us; the launch traced here: 42.6 us
  Pallas kernels  41 us (96%)
  local copies, waits for them, and re-layouts  1.62 us (4%)
    pallas_call x1, Pallas kernels, fused(): pl.pallas_call(functools.partial(kernel, nh), out_shape=jax.ShapeDtypeStr...  41 us
    unnamed x1, local copies, waits for them, and re-layouts  1.62 us

profile of v3, /device:TPU:0, one launch (start us, length us, event | category | flops | bytes accessed | tf_op | source)
XLA Modules:
  0.0 42.6 jit_solution(6316085662573291580)
XLA Ops:
  0.0 41.0 %shard_map.73 = bf16[48,2048]{1,0:T(8,128)(2,1)} custom-call(f32[4]{0:T(128)} %mix_ref.1, f32[1,128]{1,0:T(1,128)} %bitcast.1, bf16[48,2048]{1,0:T(8,128)(2,1)} %tok_ref.1, bf16[2048,512]{1,0:T(8,128)(2,1)} %wq_hbm.1, bf16[2048,512]{1,0:T(8,128)(2,1)} %wk_hbm.1, bf16[2048,512]{1,0:T(8,128)(2,1)} %wv_hbm.1, bf16[512,2048]{1,0:T(8,128)(2,1)} %wo_hbm.1), custom_call_target="tpu_custom_call" | custom-call | tf_op jit(solution)/shard_map/pallas_call | solution.py:306
  41.0 1.6 %copy.9 = bf16[48,2048]{1,0:T(8,128)(2,1)} copy(bf16[48,2048]{1,0:T(8,128)(2,1)} %shard_map.73) | data formatting | bytes 393216

commit v4 on v3

--- a/solution.py
+++ b/solution.py
@@ -142,20 +142,28 @@
                 snd[hh, i, pl.ds(u * rows, rows), :] = y[:, hh * vd : (hh + 1) * vd]
         rcv[:, at(u, 0), :] = snd[h, :, pl.ds(u * rows, rows), :]
 
-    def send(u):
-        mine = pl.ds(u * rows, rows)
-        for copies, i, n, sem in ((z_copies, 1, 2, 0), (q_copies, 0, 1, 1)):
-            for d in range(1, nh):
-                copies[u, d] = remote(
-                    snd.at[lax.rem(h + d, nh), pl.ds(i, n), mine, :],
-                    rcv.at[pl.ds(i, n), at(u, d), :],
-                    z_ss.at[sem, u, d - 1],
-                    z_rs.at[sem, u, d - 1],
-                    head_peer(d),
-                )
-                copies[u, d].start()
+    def spread(copies, u, i, n, sem):
+        for d in range(1, nh):
+            copies[u, d] = remote(
+                snd.at[lax.rem(h + d, nh), pl.ds(i, n), pl.ds(u * rows, rows), :],
+                rcv.at[pl.ds(i, n), at(u, d), :],
+                z_ss.at[sem, u, d - 1],
+                z_rs.at[sem, u, d - 1],
+                head_peer(d),
+            )
+            copies[u, d].start()
+
+    def send_q(u):
+        spread(q_copies, u, 0, 1, 1)
+
+    def send_kv(u):
+        spread(z_copies, u, 1, 2, 0)
         x_copies[u, 0] = remote(
-            snd.at[h, pl.ds(1, 2), mine, :], kvx.at[:, at(u, 0), :], x_ss.at[u, 0], x_rs.at[u, 0], side_peer
+            snd.at[h, pl.ds(1, 2), pl.ds(u * rows, rows), :],
+            kvx.at[:, at(u, 0), :],
+            x_ss.at[u, 0],
+            x_rs.at[u, 0],
+            side_peer,
         )
         x_copies[u, 0].start()
 
@@ -220,7 +228,6 @@
             if cp == p:
                 copy.wait_recv()
 
-    project(0, tok_ref[...])
     pl.semaphore_wait(barrier, len(peers))
     to_row = remote(tok_ref, tok.at[1], a_ss.at[1], a_rs.at[1], row_peer)
     to_row.start()
@@ -228,17 +235,22 @@
     to_core.start()
     forward = remote(tok.at[1], tok.at[2], a_ss.at[2], a_rs.at[2], core_peer)
     pending += [to_row, to_core, forward]
-    send(0)
+    project(0, tok_ref[...])
+    send_kv(0)
+    send_q(0)
     to_core.wait_recv()
     project(1, tok[0])
-    send(1)
+    send_kv(1)
+    send_q(1)
     to_row.wait_recv()
     forward.start()
     project(2, tok[1])
-    send(2)
+    send_kv(2)
     forward.wait_recv()
     project(3, tok[2])
-    send(3)
+    send_kv(3)
+    send_q(2)
+    send_q(3)
     relay(0)
     relay(1)
     for u in range(2):

time: 42.7 us -> 41.6 us (0.974)
  Pallas kernels: 41 us -> 39.8 us
    pallas_call x1, Pallas kernels: 41 us -> 39.8 us  [fused(): pl.pallas_call(functools.partial(kernel, nh), out_shape=jax.ShapeDtypeStr...]
where the time goes in v4:
time: 41.6 us; the launch traced here: 41.5 us
  Pallas kernels  39.8 us (96%)
  local copies, waits for them, and re-layouts  1.62 us (4%)
    pallas_call x1, Pallas kernels, fused(): pl.pallas_call(functools.partial(kernel, nh), out_shape=jax.ShapeDtypeStr...  39.8 us
    unnamed x1, local copies, waits for them, and re-layouts  1.62 us

profile of v4, /device:TPU:0, one launch (start us, length us, event | category | flops | bytes accessed | tf_op | source)
XLA Modules:
  0.0 41.5 jit_solution(2421071290910367534)
XLA Ops:
  0.0 39.8 %shard_map.73 = bf16[48,2048]{1,0:T(8,128)(2,1)} custom-call(f32[4]{0:T(128)} %mix_ref.1, f32[1,128]{1,0:T(1,128)} %bitcast.1, bf16[48,2048]{1,0:T(8,128)(2,1)} %tok_ref.1, bf16[2048,512]{1,0:T(8,128)(2,1)} %wq_hbm.1, bf16[2048,512]{1,0:T(8,128)(2,1)} %wk_hbm.1, bf16[2048,512]{1,0:T(8,128)(2,1)} %wv_hbm.1, bf16[512,2048]{1,0:T(8,128)(2,1)} %wo_hbm.1), custom_call_target="tpu_custom_call" | custom-call | tf_op jit(solution)/shard_map/pallas_call | solution.py:318
  39.8 1.6 %copy.9 = bf16[48,2048]{1,0:T(8,128)(2,1)} copy(bf16[48,2048]{1,0:T(8,128)(2,1)} %shard_map.73) | data formatting | bytes 393216
